TPU v7x, 32 devices: a whole 2x2x4 slice. The times are simulated.
32 devices in a mesh: sp: 4 (over y, x), tp: 8 (over z, core).
Axes of the slice: x: 2, y: 2, z: 4, core: 2. Of those that a mesh axis runs over, the one named last changes fastest.
Arguments:
- resid: bfloat16 [2048, 2048], P(('sp', 'tp')), may hold values from -6 to 6
- query_a: bfloat16 [2048, 16, 128], P('sp', 'tp'), may hold values from -16 to 16
- key_a: bfloat16 [2048, 16, 128], P('sp', 'tp'), may hold values from -16 to 16
- value_a: bfloat16 [2048, 16, 128], P('sp', 'tp'), may hold values from -6 to 6
- query_b: bfloat16 [2048, 16, 64], P('sp', 'tp'), may hold values from -16 to 16
- key_b: bfloat16 [2048, 16, 64], P('sp', 'tp'), may hold values from -16 to 16
- value_b: bfloat16 [2048, 16, 64], P('sp', 'tp'), may hold values from -6 to 6
- mix_a: float32 [16], P('tp'), may hold values from 0.3 to 0.8
- mix_b: float32 [16], P('tp'), may hold values from 0.3 to 0.8
- head_gain_a: float32 [128], replicated, may hold values from 0.1 to 1.9
- head_gain_b: float32 [64], replicated, may hold values from 0.1 to 1.9
- proj_a: bfloat16 [2048, 2048], P('tp'), may hold values from -0.109375 to 0.109375
- proj_b: bfloat16 [1024, 2048], P('tp'), may hold values from -0.109375 to 0.109375
- norm_gain: float32 [2048], replicated, may hold values from 0.1 to 1.9
- route_ids: int32 [2048, 2], P(('sp', 'tp')), may hold values from 0 to 3, all different within a row; in each aligned block of 64 rows (0 to 63, 64 to 127, ...) at most 48 rows name the same one
- route_weights: float32 [2048, 2], P(('sp', 'tp')), may hold values from 0.2 to 1
- expert_gate: bfloat16 [4, 2048, 6144], P('sp', None, 'tp'), may hold values from -0.125 to 0.125
- expert_up: bfloat16 [4, 2048, 6144], P('sp', None, 'tp'), may hold values from -0.125 to 0.125
- expert_down: bfloat16 [4, 6144, 2048], P('sp', 'tp'), may hold values from -0.078125 to 0.078125
Outputs:
- out: bfloat16 [2048, 2048], P(('sp', 'tp'))
Inputs may be any that keep to these rules, and one draw needn't show every extreme that they name: `route_ids`: each row names 2 different experts. Within the rows of one device (aligned blocks of 64 rows) no expert is named by more than 48 rows, and in every draw some device's block names some expert exactly 48 times.
All inputs are finite; a program needn't handle non-finite values.
Results may differ from a plain program's by a relative error of at most 0.02.
Values may be sent and summed in bfloat16 or wider, within the bound.
A program may use at most 128 MiB of HBM per device.

v0:
```python
import math

import jax
import jax.numpy as jnp
from jax import lax
from jax.sharding import PartitionSpec as P

EPS = 1e-06
NEG = -1e30
HEAD_SCALE = 1.0 - (0.8 - 0.6 * math.exp(-0.3))
KEY_STEP = 512


def partner(value, axis, apart):
    return lax.ppermute(value, axis, [(i, i ^ 1 << apart) for i in range(lax.axis_size(axis))])


def rms_scaled(values, gain):
    return values * lax.rsqrt(jnp.mean(values * values, axis=-1, keepdims=True) + EPS) * gain


def slot_numbers(route_rows, experts, capacity):
    count, top_count = route_rows.shape
    flat = route_rows.reshape(count * top_count)
    onehot = (flat[:, None] == jnp.arange(experts, dtype=jnp.int32)[None, :]).astype(jnp.int32)
    ranks = jnp.sum((jnp.cumsum(onehot, axis=0) - onehot) * onehot, axis=1)
    return (flat * capacity + ranks).reshape(count, top_count)


def empty_map(count, heads, width):
    return (
        jnp.zeros((count, heads, width), jnp.float32),
        jnp.full((heads, count), NEG, jnp.float32),
        jnp.zeros((heads, count), jnp.float32),
    )


def empty_group(query, value):
    return (
        empty_map(query.shape[0], query.shape[1], value.shape[2]),
        empty_map(query.shape[0], query.shape[1], value.shape[2]),
    )


def map_update(state, query, keys, values, allowed, scale):
    weighted, maximum, sums = state
    scores = jnp.einsum("qhd,khd->hqk", query, keys, preferred_element_type=jnp.float32) * scale
    scores = jnp.where(allowed[None], scores, NEG)
    fresh = jnp.maximum(maximum, jnp.max(scores, axis=2))
    weights = jnp.where(allowed[None], jnp.exp(scores - fresh[:, :, None]), 0.0)
    factor = jnp.exp(maximum - fresh)
    sums = sums * factor + jnp.sum(weights, axis=2)
    added = jnp.einsum(
        "hqk,khv->qhv", weights.astype(jnp.bfloat16), values, preferred_element_type=jnp.float32
    )
    weighted = weighted * jnp.transpose(factor)[:, :, None] + added
    return (weighted, fresh, sums)


def group_update(states, query, keys, values, allowed):
    width = query.shape[2] // 2
    scale = 1.0 / math.sqrt(width)
    return tuple(
        (
            map_update(
                states[which],
                query[:, :, which * width : (which + 1) * width],
                keys[:, :, which * width : (which + 1) * width],
                values,
                allowed,
                scale,
            )
            for which in range(2)
        )
    )


def set_update(carry, queries, pieces):
    rows_a, rows_b, query_pos = queries
    piece_key_a, piece_value_a, piece_key_b, piece_value_b = pieces
    length = piece_key_a.shape[0]
    step = math.gcd(length, KEY_STEP)
    latest = query_pos[-1]

    def inner(index, states):
        first = index * step

        def compute(current):
            keys_a = lax.dynamic_slice_in_dim(piece_key_a, first, step, 0)
            values_a = lax.dynamic_slice_in_dim(piece_value_a, first, step, 0)
            keys_b = lax.dynamic_slice_in_dim(piece_key_b, first, step, 0)
            values_b = lax.dynamic_slice_in_dim(piece_value_b, first, step, 0)
            key_pos = first + jnp.arange(step, dtype=jnp.int32)
            allowed = key_pos[None, :] <= query_pos[:, None]
            return (
                group_update(current[0], rows_a, keys_a, values_a, allowed),
                group_update(current[1], rows_b, keys_b, values_b, allowed),
            )

        return lax.cond(first <= latest, compute, lambda current: current, states)

    return lax.fori_loop(0, length // step, inner, carry)


def finish_group(states, mix, gain):
    outputs = [state[0] / jnp.transpose(state[2])[:, :, None] for state in states]
    mixed = outputs[0] - mix[None, :, None] * outputs[1]
    normed = rms_scaled(mixed, gain) * HEAD_SCALE
    return normed.astype(jnp.bfloat16).reshape(mixed.shape[0], -1)


def per_device(
    resid,
    query_a,
    key_a,
    value_a,
    query_b,
    key_b,
    value_b,
    mix_a,
    mix_b,
    head_gain_a,
    head_gain_b,
    proj_a,
    proj_b,
    norm_gain,
    route_ids,
    route_weights,
    expert_gate,
    expert_up,
    expert_down,
):
    seq_rows = query_a.shape[0]
    sp_ways = lax.axis_size("sp")
    place = lax.axis_index("sp")
    positions = place * seq_rows + jnp.arange(seq_rows, dtype=jnp.int32)
    levels = sp_ways.bit_length() - 1
    half = seq_rows // 2
    moved = jnp.concatenate(
        [query_a[half:].reshape(half, -1), query_b[half:].reshape(half, -1)], axis=1
    )
    for bit in range(levels):
        moved = partner(moved, "sp", bit)
    split_at = query_a.shape[1] * query_a.shape[2]
    far_a = moved[:, :split_at].reshape(half, query_a.shape[1], query_a.shape[2])
    far_b = moved[:, split_at:].reshape(half, query_b.shape[1], query_b.shape[2])
    far_pos = (sp_ways - 1 - place) * seq_rows + half + jnp.arange(half, dtype=jnp.int32)
    query_sets = ((query_a[:half], query_b[:half], positions[:half]), (far_a, far_b, far_pos))

    def fold_keys(carry, pieces):
        return tuple(
            (set_update(states, queries, pieces) for states, queries in zip(carry, query_sets))
        )

    initial = tuple(
        (
            (empty_group(queries[0], value_a), empty_group(queries[1], value_b))
            for queries in query_sets
        )
    )
    results = fold_keys(
        initial,
        (
            lax.all_gather(key_a, "sp", axis=0, tiled=True),
            lax.all_gather(value_a, "sp", axis=0, tiled=True),
            lax.all_gather(key_b, "sp", axis=0, tiled=True),
            lax.all_gather(value_b, "sp", axis=0, tiled=True),
        ),
    )
    finished = [
        (finish_group(states[0], mix_a, head_gain_a), finish_group(states[1], mix_b, head_gain_b))
        for states in results
    ]
    returned = jnp.concatenate([finished[1][0], finished[1][1]], axis=1)
    for bit in range(levels):
        returned = partner(returned, "sp", bit)
    width_a = finished[0][0].shape[1]
    heads_out_a = jnp.concatenate([finished[0][0], returned[:, :width_a]], axis=0)
    heads_out_b = jnp.concatenate([finished[0][1], returned[:, width_a:]], axis=0)
    width = resid.shape[1]
    tok_rows = resid.shape[0]
    top_count = route_ids.shape[1]
    capacity = 3 * top_count * tok_rows // (2 * sp_ways)
    own_slots = slot_numbers(route_ids, sp_ways, capacity)
    term = jnp.dot(heads_out_a, proj_a, preferred_element_type=jnp.float32)
    term = term + jnp.dot(heads_out_b, proj_b, preferred_element_type=jnp.float32)
    mixed = resid.astype(jnp.float32) + lax.psum_scatter(
        lax.optimization_barrier(term.astype(jnp.bfloat16))
        .astype(jnp.float32)
        .astype(jnp.bfloat16),
        "tp",
        scatter_dimension=0,
        tiled=True,
    ).astype(jnp.float32)
    normed = rms_scaled(mixed, norm_gain).astype(jnp.bfloat16)
    lookup = jnp.arange(sp_ways * capacity, dtype=jnp.int32)[:, None]
    spread = jnp.zeros((sp_ways * capacity, tok_rows), jnp.float32)
    for which in range(top_count):
        spread = spread + (own_slots[:, which][None, :] == lookup).astype(jnp.float32)
    outgoing = jnp.dot(
        spread.astype(jnp.bfloat16), normed, preferred_element_type=jnp.float32
    ).astype(jnp.bfloat16)
    arrived = lax.all_to_all(
        outgoing.reshape(sp_ways, capacity, width), "sp", split_axis=0, concat_axis=0, tiled=True
    )
    piece = lax.all_gather(arrived.reshape(sp_ways * capacity, width), "tp", axis=0, tiled=True)
    gate = jnp.dot(piece, expert_gate[0], preferred_element_type=jnp.float32)
    upward = jnp.dot(piece, expert_up[0], preferred_element_type=jnp.float32)
    hidden = (jax.nn.silu(gate) * upward).astype(jnp.bfloat16)
    term = jnp.dot(hidden, expert_down[0], preferred_element_type=jnp.float32)
    summed = lax.psum_scatter(
        lax.optimization_barrier(term.astype(jnp.bfloat16))
        .astype(jnp.float32)
        .astype(jnp.bfloat16),
        "tp",
        scatter_dimension=0,
        tiled=True,
    )
    finished_rows = summed.reshape(sp_ways, capacity, width)
    back = lax.all_to_all(finished_rows, "sp", split_axis=0, concat_axis=0, tiled=True)
    picked = jnp.take(back.reshape(sp_ways * capacity, width), own_slots.reshape(-1), axis=0)
    picked = picked.reshape(tok_rows, top_count, width)
    output = mixed + jnp.sum(route_weights[:, :, None] * picked.astype(jnp.float32), axis=1)
    return output.astype(jnp.bfloat16)


def solution(mesh):
    placed = (
        P(("sp", "tp"), None),
        P("sp", "tp", None),
        P("sp", "tp", None),
        P("sp", "tp", None),
        P("sp", "tp", None),
        P("sp", "tp", None),
        P("sp", "tp", None),
        P("tp"),
        P("tp"),
        P(),
        P(),
        P("tp", None),
        P("tp", None),
        P(),
        P(("sp", "tp"), None),
        P(("sp", "tp"), None),
        P("sp", None, "tp"),
        P("sp", None, "tp"),
        P("sp", "tp", None),
    )
    return jax.shard_map(
        per_device, mesh=mesh, in_specs=placed, out_specs=P(("sp", "tp"), None), check_vma=False
    )
```

profile of v0, /device:TPU:0, one launch (start us, length us, event | category | flops | bytes accessed | tf_op | source)
XLA Modules:
  0.0 423.4 jit_solution(7599969802928675392)
XLA Ops:
  14.0 3.0 collective-permute-start
  19.5 4.5 %collective-permute-done = bf16[256,384]{0,1:T(8,128)(2,1)} collective-permute-done((bf16[256,384]{0,1:T(8,128)(2,1)}, bf16[256,384]{0,1:T(8,128)(2,1)}, u32[]{:S(2)}, u32[]{:S(2)}) %collective-permute-start) | collective-permute-done | bytes 196640 | tf_op jit(solution)/shard_map/ppermute | solution.py:15
  25.3 16.1 %all_gather.17 = bf16[2048,2,64]{0,2,1:T(8,128)(2,1)} all-gather(bf16[512,2,64]{0,2,1:T(8,128)(2,1)} %param.32), channel_id=1, replica_groups=mesh['sp'=4,'tp'=8] {'sp'}, dimensions={0}, use_global_device_ids=true | all-gather | bytes 655360 | tf_op jit(solution)/shard_map/all_gather | solution.py:166
  41.4 10.7 %all_gather.18 = bf16[2048,2,64]{0,2,1:T(8,128)(2,1)} all-gather(bf16[512,2,64]{0,2,1:T(8,128)(2,1)} %param.33), channel_id=1, replica_groups=mesh['sp'=4,'tp'=8] {'sp'}, dimensions={0}, use_global_device_ids=true | all-gather | bytes 655360 | tf_op jit(solution)/shard_map/all_gather | solution.py:167
  53.4 17.1 %all-gather.6.cloned.1.call-done = bf16[2048,2,128]{0,2,1:T(8,128)(2,1)} async-done(((bf16[512,2,128]{0,2,1:T(8,128)(2,1)}), bf16[2048,2,128]{0,2,1:T(8,128)(2,1)}) %all-gather.6.cloned.1.call-update) | async-done | bytes 1048592 | tf_op jit(solution)/shard_map/all_gather | solution.py:165
  74.9 65.4 %while.72 = (s32[]{:T(128)}, f32[256,2,128]{0,2,1:T(8,128)S(1)}, f32[2,256]{1,0:T(2,128)S(1)}, f32[2,256]{1,0:T(2,128)}, f32[256,2,128]{0,2,1:T(8,128)}, /*index...) while((s32[]{:T(128)}, f32[256,2,128]{0,2,1:T(8,128)S(1)}, ...), condition=%wide.region_24.25_spmd.clone, body=%wide.region_13.24_spmd.clone.sunk | while | flops 311958272 | bytes 29590432 | solution.py:102
  75.5 15.7 %conditional.6 = ((f32[256,2,128]{0,2,1:T(8,128)S(1)}, f32[2,256]{1,0:T(2,128)S(1)}, f32[2,256]{1,0:T(2,128)}, f32[256,2,128]{0,2,1:T(8,128)}, f32[2,256]{1,0:T(...) conditional(s32[]{:T(128)} %convert_element_type.167, ...), branch_computations={%region_14.14_spmd, %region_15.23_spmd} | conditional | flops 311958272 | bytes 29588914 | solution.py:100
  75.7 2.3 fusion.157
  91.8 15.8 %conditional.6 = ((f32[256,2,128]{0,2,1:T(8,128)S(1)}, f32[2,256]{1,0:T(2,128)S(1)}, f32[2,256]{1,0:T(2,128)}, f32[256,2,128]{0,2,1:T(8,128)}, f32[2,256]{1,0:T(...) conditional(s32[]{:T(128)} %convert_element_type.167, ...), branch_computations={%region_14.14_spmd, %region_15.23_spmd} | conditional | flops 311958272 | bytes 29588914 | solution.py:100
  92.0 2.2 fusion.157
  108.2 15.7 %conditional.6 = ((f32[256,2,128]{0,2,1:T(8,128)S(1)}, f32[2,256]{1,0:T(2,128)S(1)}, f32[2,256]{1,0:T(2,128)}, f32[256,2,128]{0,2,1:T(8,128)}, f32[2,256]{1,0:T(...) conditional(s32[]{:T(128)} %convert_element_type.167, ...), branch_computations={%region_14.14_spmd, %region_15.23_spmd} | conditional | flops 311958272 | bytes 29588914 | solution.py:100
  108.4 2.2 fusion.157
  124.5 15.7 %conditional.6 = ((f32[256,2,128]{0,2,1:T(8,128)S(1)}, f32[2,256]{1,0:T(2,128)S(1)}, f32[2,256]{1,0:T(2,128)}, f32[256,2,128]{0,2,1:T(8,128)}, f32[2,256]{1,0:T(...) conditional(s32[]{:T(128)} %convert_element_type.167, ...), branch_computations={%region_14.14_spmd, %region_15.23_spmd} | conditional | flops 311958272 | bytes 29588914 | solution.py:100
  124.7 2.2 fusion.157
  145.4 19.4 %while.71 = (s32[]{:T(128)}, f32[256,2,128]{0,2,1:T(8,128)S(1)}, f32[2,256]{1,0:T(2,128)S(1)}, f32[2,256]{1,0:T(2,128)}, f32[256,2,128]{0,2,1:T(8,128)}, /*index...) while((s32[]{:T(128)}, f32[256,2,128]{0,2,1:T(8,128)S(1)}, ...), condition=%wide.region_11.12_spmd, body=%wide.region_0.11_spmd.sunk | while | flops 311958016 | bytes 29587348 | solution.py:102
  146.0 16.9 %conditional.5 = ((f32[256,2,128]{0,2,1:T(8,128)S(1)}, f32[2,256]{1,0:T(2,128)S(1)}, f32[2,256]{1,0:T(2,128)}, f32[256,2,128]{0,2,1:T(8,128)}, f32[2,256]{1,0:T(...) conditional(s32[]{:T(128)} %convert_element_type.166, ...), branch_computations={%region_1.0_spmd, %region_2.10_spmd} | conditional | flops 311958016 | bytes 29586862 | solution.py:100
  147.4 2.3 fusion.153
  169.0 2.7 collective-permute-start.2
  171.8 4.7 %collective-permute-done.2 = bf16[256,384]{0,1:T(8,128)(2,1)S(1)} collective-permute-done((bf16[256,384]{0,1:T(8,128)(2,1)S(1)}, bf16[256,384]{0,1:T(8,128)(2,1)S(1)}, u32[]{:S(2)}, u32[]{:S(2)}) %collective-permute-start.2) | collective-permute-done | bytes 196640 | tf_op jit(solution)/shard_map/ppermute | solution.py:15
  176.5 3.0 collective-permute-start.3
  179.4 3.9 collective-permute-done.3
  187.2 36.5 %reduce-scatter.3.cloned.1.call-done = bf16[64,2048]{1,0:T(8,128)(2,1)} async-done(((bf16[512,2048]{1,0:T(8,128)(2,1)}), bf16[64,2048]{1,0:T(8,128)(2,1)}) %reduce-scatter.3.cloned.1.call-update) | async-done | bytes 262160 | tf_op jit(solution)/shard_map/reduce_scatter | solution.py:187
  226.3 12.3 %all_to_all.10 = bf16[4,48,2048]{2,1,0:T(8,128)(2,1)} all-to-all(bf16[4,48,2048]{2,1,0:T(8,128)(2,1)S(1)} %bitcast.127), channel_id=1, replica_groups=mesh['sp'=4,'tp'=8] {'sp'}, dimensions={0} | all-to-all | bytes 1572864 | tf_op jit(solution)/shard_map/all_to_all | solution.py:203
  238.8 63.9 %all-gather.8.cloned.1.call-done = bf16[1536,2048]{1,0:T(8,128)(2,1)} async-done(((bf16[192,2048]{1,0:T(8,128)(2,1)}), bf16[1536,2048]{1,0:T(8,128)(2,1)}) %all-gather.8.cloned.1.call-update) | async-done | bytes 6291472 | tf_op jit(solution)/shard_map/all_gather | solution.py:206
  302.7 8.2 %fusion.132 = f32[1536,768]{1,0:T(8,128)S(1)} fusion(bf16[1536,2048]{1,0:T(8,128)(2,1)} %all-gather.8.cloned.1.call-done, bf16[1,2048,768]{2,1,0:T(8,128)(2,1)} %param.43), kind=kOutput, calls=%fused_computation.172 | convolution fusion | flops 4831838208 | bytes 14155776 | tf_op jit(solution)/shard_map/dot_general | solution.py:207
  311.0 5.6 %multiply_convert_fusion = bf16[1536,768]{1,0:T(8,128)(2,1)S(1)} fusion(f32[1536,768]{1,0:T(8,128)S(1)} %fusion.132, bf16[1536,2048]{1,0:T(8,128)(2,1)S(1)} %copy-done.24, bf16[1,2048,768]{2,1,0:T(8,128)(2,1)S(1)} %copy-done.25), kind=kOutput, calls=%fused_computation.168 | convolution fusion | flops 4838916096 | bytes 16515072 | tf_op jit(solution)/shard_map/dot_general | solution.py:208
  316.6 7.1 %convolution_convert_fusion = bf16[1536,2048]{1,0:T(8,128)(2,1)} fusion(bf16[1536,768]{1,0:T(8,128)(2,1)S(1)} %multiply_convert_fusion, bf16[1,768,2048]{2,1,0:T(8,128)(2,1)S(1)} %copy-done), kind=kOutput, calls=%fused_computation.167 | convolution fusion | flops 4834983936 | bytes 11796480 | tf_op jit(solution)/shard_map/dot_general | solution.py:210
  323.7 68.5 %reduce-scatter.5.cloned.1.call-done = bf16[192,2048]{1,0:T(8,128)(2,1)} async-done(((bf16[1536,2048]{1,0:T(8,128)(2,1)}), bf16[192,2048]{1,0:T(8,128)(2,1)}) %reduce-scatter.5.cloned.1.call-update) | async-done | bytes 786448 | tf_op jit(solution)/shard_map/reduce_scatter | solution.py:211
  392.3 4.2 all-to-all-start.1
  396.9 8.8 %all-to-all-done.1 = bf16[4,48,2048]{2,1,0:T(8,128)(2,1)} async-done(((bf16[4,48,2048]{2,1,0:T(8,128)(2,1)}), bf16[4,48,2048]{2,1,0:T(8,128)(2,1)}, u32[]{:S(2)}, u32[]{:S(2)}) %all-to-all-start.1) | async-done | bytes 786464 | tf_op jit(solution)/shard_map/all_to_all | solution.py:220
  405.7 3.5 gather_fusion
  411.4 3.7 multiply_reduce_fusion
  (294 shorter events, 104.9 us)
Async XLA Ops:
  6.5 310.0 %copy-start = (bf16[1,768,2048]{2,1,0:T(8,128)(2,1)S(1)}, bf16[1,768,2048]{2,1,0:T(8,128)(2,1)}, u32[]{:S(2)}) copy-start(bf16[1,768,2048]{2,1,0:T(8,128)(2,1)} %param.45) | copy-start | bytes 9437188
  6.5 46.9 %all-gather.4.cloned.1.call-start = ((), (), s32[]{:S(2)}) async-start(), calls=%async_computation.4 | async-start | bytes 1310720 | tf_op jit(solution)/shard_map/all_gather | solution.py:164
  8.5 62.0 %all-gather.6.cloned.1.call-start = ((), (), s32[]{:S(2)}) async-start(), calls=%async_computation.5 | async-start | bytes 1310720 | tf_op jit(solution)/shard_map/all_gather | solution.py:165
  10.4 213.3 %reduce-scatter.3.cloned.1.call-start = ((), (), s32[]{:S(2)}) async-start(), calls=%async_computation.6 | async-start | bytes 2359296 | tf_op jit(solution)/shard_map/reduce_scatter | solution.py:187
  14.0 10.0 %collective-permute-start = (bf16[256,384]{0,1:T(8,128)(2,1)}, bf16[256,384]{0,1:T(8,128)(2,1)}, u32[]{:S(2)}, u32[]{:S(2)}) collective-permute-start(bf16[256,384]{0,1:T(8,128)(2,1)} %pad_maximum_fusion), channel_id=1, source_target_pairs={{0,8},{8,0},{16,24},{24,16},{1,9},{9,1},{17,25},{25,17},{2,10},{10... | collective-permute-start | bytes 589832 | tf_op jit(solution)/shard_map/ppermute | solution.py:15
  24.0 28.1 %collective-permute-start.1 = (bf16[256,384]{0,1:T(8,128)(2,1)}, bf16[256,384]{0,1:T(8,128)(2,1)S(1)}, u32[]{:S(2)}, u32[]{:S(2)}) collective-permute-start(bf16[256,384]{0,1:T(8,128)(2,1)} %collective-permute-done), channel_id=1, source_target_pairs={{0,16},{8,24},{16,0},{24,8},{1,17},{9,25},{17,1},{25,9},{2,18},{10... | collective-permute-start | bytes 589832 | tf_op jit(solution)/shard_map/ppermute | solution.py:15
  78.5 8.0 %copy-start.3 = (bf16[2048,2,128]{0,2,1:T(8,128)(2,1)S(1)}, bf16[2048,2,128]{0,2,1:T(8,128)(2,1)}, u32[]{:S(2)}) copy-start(bf16[2048,2,128]{0,2,1:T(8,128)(2,1)} %get-tuple-element.863) | copy-start | bytes 3145732 | tf_op jit(solution)/shard_map/while/body/eval_jaxpr/cond
  78.5 8.0 %copy-start.10 = (f32[256,2,128]{0,2,1:T(8,128)S(1)}, f32[256,2,128]{0,2,1:T(8,128)}, u32[]{:S(2)}) copy-start(f32[256,2,128]{0,2,1:T(8,128)} %get-tuple-element.865) | copy-start | bytes 786436 | tf_op jit(solution)/shard_map/while/body/eval_jaxpr/cond
  78.6 8.0 %copy-start.19 = (f32[256,2]{0,1:T(2,128)S(1)}, f32[256,2]{0,1:T(2,128)}, u32[]{:S(2)}) copy-start(f32[256,2]{0,1:T(2,128)} %get-tuple-element.1107) | copy-start | bytes 6148 | tf_op jit(solution)/shard_map/while/body/eval_jaxpr/cond
  94.9 8.0 %copy-start.3 = (bf16[2048,2,128]{0,2,1:T(8,128)(2,1)S(1)}, bf16[2048,2,128]{0,2,1:T(8,128)(2,1)}, u32[]{:S(2)}) copy-start(bf16[2048,2,128]{0,2,1:T(8,128)(2,1)} %get-tuple-element.863) | copy-start | bytes 3145732 | tf_op jit(solution)/shard_map/while/body/eval_jaxpr/cond
  94.9 8.0 %copy-start.10 = (f32[256,2,128]{0,2,1:T(8,128)S(1)}, f32[256,2,128]{0,2,1:T(8,128)}, u32[]{:S(2)}) copy-start(f32[256,2,128]{0,2,1:T(8,128)} %get-tuple-element.865) | copy-start | bytes 786436 | tf_op jit(solution)/shard_map/while/body/eval_jaxpr/cond
  94.9 8.0 %copy-start.19 = (f32[256,2]{0,1:T(2,128)S(1)}, f32[256,2]{0,1:T(2,128)}, u32[]{:S(2)}) copy-start(f32[256,2]{0,1:T(2,128)} %get-tuple-element.1107) | copy-start | bytes 6148 | tf_op jit(solution)/shard_map/while/body/eval_jaxpr/cond
  111.2 8.0 %copy-start.3 = (bf16[2048,2,128]{0,2,1:T(8,128)(2,1)S(1)}, bf16[2048,2,128]{0,2,1:T(8,128)(2,1)}, u32[]{:S(2)}) copy-start(bf16[2048,2,128]{0,2,1:T(8,128)(2,1)} %get-tuple-element.863) | copy-start | bytes 3145732 | tf_op jit(solution)/shard_map/while/body/eval_jaxpr/cond
  111.2 8.0 %copy-start.10 = (f32[256,2,128]{0,2,1:T(8,128)S(1)}, f32[256,2,128]{0,2,1:T(8,128)}, u32[]{:S(2)}) copy-start(f32[256,2,128]{0,2,1:T(8,128)} %get-tuple-element.865) | copy-start | bytes 786436 | tf_op jit(solution)/shard_map/while/body/eval_jaxpr/cond
  111.2 8.0 %copy-start.19 = (f32[256,2]{0,1:T(2,128)S(1)}, f32[256,2]{0,1:T(2,128)}, u32[]{:S(2)}) copy-start(f32[256,2]{0,1:T(2,128)} %get-tuple-element.1107) | copy-start | bytes 6148 | tf_op jit(solution)/shard_map/while/body/eval_jaxpr/cond
  127.6 8.0 %copy-start.3 = (bf16[2048,2,128]{0,2,1:T(8,128)(2,1)S(1)}, bf16[2048,2,128]{0,2,1:T(8,128)(2,1)}, u32[]{:S(2)}) copy-start(bf16[2048,2,128]{0,2,1:T(8,128)(2,1)} %get-tuple-element.863) | copy-start | bytes 3145732 | tf_op jit(solution)/shard_map/while/body/eval_jaxpr/cond
  127.6 8.0 %copy-start.10 = (f32[256,2,128]{0,2,1:T(8,128)S(1)}, f32[256,2,128]{0,2,1:T(8,128)}, u32[]{:S(2)}) copy-start(f32[256,2,128]{0,2,1:T(8,128)} %get-tuple-element.865) | copy-start | bytes 786436 | tf_op jit(solution)/shard_map/while/body/eval_jaxpr/cond
  127.6 8.0 %copy-start.19 = (f32[256,2]{0,1:T(2,128)S(1)}, f32[256,2]{0,1:T(2,128)}, u32[]{:S(2)}) copy-start(f32[256,2]{0,1:T(2,128)} %get-tuple-element.1107) | copy-start | bytes 6148 | tf_op jit(solution)/shard_map/while/body/eval_jaxpr/cond
  150.2 8.0 %copy-start.4 = (bf16[2048,2,128]{0,2,1:T(8,128)(2,1)S(1)}, bf16[2048,2,128]{0,2,1:T(8,128)(2,1)}, u32[]{:S(2)}) copy-start(bf16[2048,2,128]{0,2,1:T(8,128)(2,1)} %get-tuple-element.809) | copy-start | bytes 3145732 | tf_op jit(solution)/shard_map/while/body/eval_jaxpr/cond
  150.2 8.0 %copy-start.7 = (f32[256,2,128]{0,2,1:T(8,128)S(1)}, f32[256,2,128]{0,2,1:T(8,128)}, u32[]{:S(2)}) copy-start(f32[256,2,128]{0,2,1:T(8,128)} %get-tuple-element.811) | copy-start | bytes 786436 | tf_op jit(solution)/shard_map/while/body/eval_jaxpr/cond
  164.7 18.6 %copy-start.14 = (bf16[128,2048]{1,0:T(8,128)(2,1)S(1)}, bf16[128,2048]{1,0:T(8,128)(2,1)}, u32[]{:S(2)}) copy-start(bf16[128,2048]{1,0:T(8,128)(2,1)} %param.39) | copy-start | bytes 1572868
  166.1 18.0 %copy-start.13 = (bf16[256,2048]{1,0:T(8,128)(2,1)S(1)}, bf16[256,2048]{1,0:T(8,128)(2,1)}, u32[]{:S(2)}) copy-start(bf16[256,2048]{1,0:T(8,128)(2,1)} %param.38) | copy-start | bytes 3145732
  169.0 7.5 %collective-permute-start.2 = (bf16[256,384]{0,1:T(8,128)(2,1)S(1)}, bf16[256,384]{0,1:T(8,128)(2,1)S(1)}, u32[]{:S(2)}, u32[]{:S(2)}) collective-permute-start(bf16[256,384]{0,1:T(8,128)(2,1)S(1)} %pad_maximum_fusion.1), channel_id=1, source_target_pairs={{0,8},{8,0},{16,24},{24,16},{1,9},{9,1},{17,25},{25,17},{2,10},{10... | collective-permute-start | bytes 589832 | tf_op jit(solution)/shard_map/ppermute | solution.py:15
  176.5 6.9 %collective-permute-start.3 = (bf16[256,384]{0,1:T(8,128)(2,1)S(1)}, bf16[256,384]{0,1:T(8,128)(2,1)S(1)}, u32[]{:S(2)}, u32[]{:S(2)}) collective-permute-start(bf16[256,384]{0,1:T(8,128)(2,1)S(1)} %collective-permute-done.2), channel_id=1, source_target_pairs={{0,16},{8,24},{16,0},{24,8},{1,17},{9,25},{17,1},{25,9},{2,18},{10... | collective-permute-start | bytes 589832 | tf_op jit(solution)/shard_map/ppermute | solution.py:15
  184.1 39.6 %copy-start.12 = (bf16[64,2048]{1,0:T(8,128)(2,1)S(1)}, bf16[64,2048]{1,0:T(8,128)(2,1)}, u32[]{:S(2)}) copy-start(bf16[64,2048]{1,0:T(8,128)(2,1)} %param.27) | copy-start | bytes 786436
  184.1 40.8 %copy-start.22 = (f32[2048]{0:T(1024)S(1)}, f32[2048]{0:T(1024)}, u32[]{:S(2)}) copy-start(f32[2048]{0:T(1024)} %param.40) | copy-start | bytes 24580
  186.3 116.5 %all-gather.8.cloned.1.call-start = ((), (), s32[]{:S(2)}) async-start(), calls=%async_computation.7 | async-start | bytes 7077888 | tf_op jit(solution)/shard_map/all_gather | solution.py:206
  238.6 153.7 %reduce-scatter.5.cloned.1.call-start = ((), (), s32[]{:S(2)}) async-start(), calls=%async_computation.8 | async-start | bytes 7077888 | tf_op jit(solution)/shard_map/reduce_scatter | solution.py:211
  302.7 8.2 %copy-start.24 = (bf16[1536,2048]{1,0:T(8,128)(2,1)S(1)}, bf16[1536,2048]{1,0:T(8,128)(2,1)}, u32[]{:S(2)}) copy-start(bf16[1536,2048]{1,0:T(8,128)(2,1)} %all-gather.8.cloned.1.call-done) | copy-start | bytes 18874372
  302.7 8.2 %copy-start.25 = (bf16[1,2048,768]{2,1,0:T(8,128)(2,1)S(1)}, bf16[1,2048,768]{2,1,0:T(8,128)(2,1)}, u32[]{:S(2)}) copy-start(bf16[1,2048,768]{2,1,0:T(8,128)(2,1)} %param.44) | copy-start | bytes 9437188
  323.7 73.1 %copy-start.23 = (f32[64,2]{0,1:T(2,128)S(1)}, f32[64,2]{0,1:T(2,128)}, u32[]{:S(2)}) copy-start(f32[64,2]{0,1:T(2,128)} %param.42) | copy-start | bytes 1540
  392.3 13.5 %all-to-all-start.1 = ((bf16[4,48,2048]{2,1,0:T(8,128)(2,1)}), bf16[4,48,2048]{2,1,0:T(8,128)(2,1)}, u32[]{:S(2)}, u32[]{:S(2)}) async-start(bf16[4,48,2048]{2,1,0:T(8,128)(2,1)} %bitcast.128), calls=%async_computation.3 | async-start | bytes 1572864 | tf_op jit(solution)/shard_map/all_to_all | solution.py:220
  (28 other events, 118.1 us)
Sparse Core Ops, SparseCore 0:
  9.2 32.6 all-gather.3
  43.7 26.7 all-gather.5
  186.4 37.3 reduce-scatter.2
  238.7 63.9 all-gather.7
  323.8 68.3 reduce-scatter.4
where the time goes:
time: 425 us; the launch traced here: 423 us
  waiting for transfers between devices  208 us (49%)
  matrix products  78.7 us (19%)
  blocking collectives  39.1 us (9%)
  other arithmetic  36.5 us (9%)
  local copies, waits for them, and re-layouts  27.2 us (6%)
  starting transfers between devices  14.5 us (3%)
  between operations  13.5 us (3%)
  loops' own time  5.82 us (1%)
    reduce_scatter x2, waiting for transfers between devices, per_device(): lax.psum_scatter(lax.optimization_barrier(term.astype(jnp.bfloat16)).asty...  105 us
    all_gather x1, waiting for transfers between devices, per_device(): lax.all_gather(arrived.reshape(sp_ways * capacity, width), 'tp', axis=0,...  63.9 us
    dot_general x20, matrix products, map_update(): jnp.einsum('qhd,khd->hqk', query, keys, preferred_element_type=jnp.float32)  30.7 us
    dot_general x20, matrix products, map_update(): jnp.einsum('hqk,khv->qhv', weights.astype(jnp.bfloat16), values, preferre...  22.8 us
    all_gather x1, waiting for transfers between devices, per_device(): lax.all_gather(value_a, 'sp', axis=0, tiled=True)  17.1 us
    all_gather x1, blocking collectives, per_device(): lax.all_gather(key_b, 'sp', axis=0, tiled=True)  16.1 us
    ppermute x4, waiting for transfers between devices, partner(): lax.ppermute(value, axis, [(i, i ^ 1 << apart) for i in range(lax.axis_si...  13.2 us
    add x10, other arithmetic, map_update(): sums = sums * factor + jnp.sum(weights, axis=2)  12.9 us
  transfers between devices with their start and end apart: 10, of which 8 were waited for; matrix products, arithmetic and copies ran while one was open for 2% of the time, Pallas kernels for 0%

commit v1 on v0

--- a/solution.py
+++ b/solution.py
@@ -1,8 +1,11 @@
+import functools
 import math
 
 import jax
 import jax.numpy as jnp
 from jax import lax
+from jax.experimental import pallas as pl
+from jax.experimental.pallas import tpu as pltpu
 from jax.sharding import PartitionSpec as P
 
 EPS = 1e-06
@@ -107,6 +110,230 @@
     mixed = outputs[0] - mix[None, :, None] * outputs[1]
     normed = rms_scaled(mixed, gain) * HEAD_SCALE
     return normed.astype(jnp.bfloat16).reshape(mixed.shape[0], -1)
+
+
+def greet(axis, ways):
+    me = lax.axis_index(axis)
+    barrier = pltpu.get_barrier_semaphore()
+    for apart in range(1, ways):
+        pl.semaphore_signal(
+            barrier,
+            inc=1,
+            device_id={axis: lax.rem(me + apart, ways)},
+            device_id_type=pl.DeviceIdType.MESH,
+        )
+    pl.semaphore_wait(barrier, ways - 1)
+
+
+def heads_kernel(
+    ways, chunk, x_ref, par_ref, out_ref, got, heads, send_in, recv_in, send_out, recv_out
+):
+    me = lax.axis_index("sp")
+    rows, wide = got.shape[1], out_ref.shape[2]
+    greet("sp", ways)
+    arriving = []
+    for apart in range(1, ways):
+        peer = lax.rem(me + apart, ways)
+        copy = pltpu.make_async_remote_copy(
+            src_ref=x_ref.at[peer],
+            dst_ref=got.at[me],
+            send_sem=send_in.at[apart],
+            recv_sem=recv_in.at[apart],
+            device_id={"sp": peer},
+            device_id_type=pl.DeviceIdType.MESH,
+        )
+        copy.start()
+        arriving.append(copy)
+    got[me] = x_ref[me]
+    for copy in arriving:
+        copy.wait()
+    gain, mix = par_ref[0:1, :], par_ref[1:2, :]
+    scale, share = par_ref[2:3, 0:1], par_ref[3:4, 0:1]
+    lane = lax.broadcasted_iota(jnp.int32, (chunk, wide), 1)
+
+    def result_copy(block):
+        return pltpu.make_async_remote_copy(
+            src_ref=heads.at[block],
+            dst_ref=out_ref.at[me],
+            send_sem=send_out.at[block],
+            recv_sem=recv_out.at[me],
+            device_id={"sp": block},
+            device_id_type=pl.DeviceIdType.MESH,
+        )
+
+    for block in reversed(range(ways)):
+        length = (block + 1) * rows
+
+        @pl.loop(0, rows // chunk)
+        def _(step):
+            first = pl.multiple_of(step * chunk, chunk)
+            query = got[block, pl.ds(first, chunk), 0:wide]
+            keys = got[0 : block + 1, :, wide : 2 * wide].reshape(length, wide)
+            values = got[0 : block + 1, :, 2 * wide : 3 * wide].reshape(length, wide)
+            row = first + block * rows + lax.broadcasted_iota(jnp.int32, (chunk, rows), 0)
+            col = block * rows + lax.broadcasted_iota(jnp.int32, (chunk, rows), 1)
+            parts = []
+            for which in range(2):
+                own = (lane < wide // 2) if which == 0 else (lane >= wide // 2)
+                picked = jnp.where(own, query, jnp.zeros_like(query))
+                scores = lax.dot_general(
+                    picked, keys, (((1,), (1,)), ((), ())), preferred_element_type=jnp.float32
+                )
+                last = jnp.where(col <= row, scores[:, block * rows :], NEG)
+                if block:
+                    scores = jnp.concatenate([scores[:, : block * rows], last], axis=1)
+                else:
+                    scores = last
+                top = jnp.max(scores, axis=1, keepdims=True)
+                weights = jnp.exp2((scores - top) * scale)
+                sums = jnp.sum(weights, axis=1, keepdims=True)
+                mixed = jnp.dot(
+                    weights.astype(jnp.bfloat16), values, preferred_element_type=jnp.float32
+                )
+                parts.append(mixed / sums)
+            mixed = parts[0] - mix * parts[1]
+            square = jnp.sum(mixed * mixed, axis=1, keepdims=True) * share
+            heads[block, pl.ds(first, chunk), :] = (
+                mixed * lax.rsqrt(square + EPS) * gain * HEAD_SCALE
+            ).astype(jnp.bfloat16)
+
+        @pl.when(me != block)
+        def _():
+            result_copy(block).start()
+
+        @pl.when(me == block)
+        def _():
+            out_ref[block] = heads[block]
+
+    for block in range(ways):
+
+        @pl.when(me != block)
+        def _():
+            result_copy(block).wait_send()
+            pltpu.make_async_remote_copy(
+                src_ref=heads.at[block],
+                dst_ref=out_ref.at[block],
+                send_sem=send_out.at[block],
+                recv_sem=recv_out.at[block],
+                device_id={"sp": block},
+                device_id_type=pl.DeviceIdType.MESH,
+            ).wait_recv()
+
+
+def wide_head(query, keys, values, wide, value_wide):
+    rows, narrow = query.shape[0], query.shape[1] // 2
+
+    def maps(array):
+        halves = array.reshape(rows, 2, narrow)
+        return jnp.pad(halves, ((0, 0), (0, 0), (0, wide - narrow))).reshape(rows, 2 * wide)
+
+    padded = jnp.pad(values, ((0, 0), (0, value_wide - values.shape[1])))
+    return jnp.concatenate([maps(query), maps(keys), padded], axis=1)
+
+
+def whole_heads(query_a, key_a, value_a, query_b, key_b, value_b, mix_a, mix_b, gain_a, gain_b):
+    ways = lax.axis_size("sp")
+    heads_a, heads_b = query_a.shape[1], query_b.shape[1]
+    rows, wide = query_a.shape[0], value_a.shape[2]
+    half = query_a.shape[2] // 2
+    order = [("a", h) for h in range(heads_a)]
+    spot = heads_a // 2
+    order = order[:spot] + [("b", h) for h in range(heads_b)] + order[spot:]
+    units, params = [], []
+    for group, head in order:
+        if group == "a":
+            query, keys, values, mix, gain = query_a, key_a, value_a, mix_a, gain_a
+        else:
+            query, keys, values, mix, gain = query_b, key_b, value_b, mix_b, gain_b
+        units.append(wide_head(query[:, head], keys[:, head], values[:, head], half, wide))
+        value_wide = values.shape[2]
+        scale = math.log2(math.e) / math.sqrt(query.shape[2] // 2)
+        params.append(
+            jnp.stack(
+                [
+                    jnp.pad(gain, (0, wide - value_wide)),
+                    jnp.full((wide,), mix[head]),
+                    jnp.full((wide,), scale, jnp.float32),
+                    jnp.full((wide,), 1.0 / value_wide, jnp.float32),
+                ]
+            )
+        )
+    par = lax.dynamic_index_in_dim(
+        jnp.stack(params), lax.axis_index("sp"), axis=0, keepdims=False
+    )
+    chunk = math.gcd(rows, 128)
+    got = pl.pallas_call(
+        functools.partial(heads_kernel, ways, chunk),
+        out_shape=jax.ShapeDtypeStruct((ways, rows, wide), jnp.bfloat16),
+        in_specs=[pl.BlockSpec(memory_space=pltpu.VMEM)] * 2,
+        out_specs=pl.BlockSpec(memory_space=pltpu.VMEM),
+        scratch_shapes=[
+            pltpu.VMEM((ways, rows, 3 * wide), jnp.bfloat16),
+            pltpu.VMEM((ways, rows, wide), jnp.bfloat16),
+            pltpu.SemaphoreType.DMA((ways,)),
+            pltpu.SemaphoreType.DMA((ways,)),
+            pltpu.SemaphoreType.DMA((ways,)),
+            pltpu.SemaphoreType.DMA((ways,)),
+        ],
+        compiler_params=pltpu.CompilerParams(
+            collective_id=1, has_side_effects=True, vmem_limit_bytes=48 << 20
+        ),
+    )(jnp.stack(units), jnp.pad(par, ((0, 4), (0, 0))))
+    out_a = [got[at] for at, unit in enumerate(order) if unit[0] == "a"]
+    out_b = [got[at, :, : value_b.shape[2]] for at, unit in enumerate(order) if unit[0] == "b"]
+    return jnp.concatenate(out_a, axis=1), jnp.concatenate(out_b, axis=1)
+
+
+def zigzag_heads(query_a, key_a, value_a, query_b, key_b, value_b, mix_a, mix_b, gain_a, gain_b):
+    head_gain_a, head_gain_b = gain_a, gain_b
+    seq_rows = query_a.shape[0]
+    sp_ways = lax.axis_size("sp")
+    place = lax.axis_index("sp")
+    positions = place * seq_rows + jnp.arange(seq_rows, dtype=jnp.int32)
+    levels = sp_ways.bit_length() - 1
+    half = seq_rows // 2
+    moved = jnp.concatenate(
+        [query_a[half:].reshape(half, -1), query_b[half:].reshape(half, -1)], axis=1
+    )
+    for bit in range(levels):
+        moved = partner(moved, "sp", bit)
+    split_at = query_a.shape[1] * query_a.shape[2]
+    far_a = moved[:, :split_at].reshape(half, query_a.shape[1], query_a.shape[2])
+    far_b = moved[:, split_at:].reshape(half, query_b.shape[1], query_b.shape[2])
+    far_pos = (sp_ways - 1 - place) * seq_rows + half + jnp.arange(half, dtype=jnp.int32)
+    query_sets = ((query_a[:half], query_b[:half], positions[:half]), (far_a, far_b, far_pos))
+
+    def fold_keys(carry, pieces):
+        return tuple(
+            (set_update(states, queries, pieces) for states, queries in zip(carry, query_sets))
+        )
+
+    initial = tuple(
+        (
+            (empty_group(queries[0], value_a), empty_group(queries[1], value_b))
+            for queries in query_sets
+        )
+    )
+    results = fold_keys(
+        initial,
+        (
+            lax.all_gather(key_a, "sp", axis=0, tiled=True),
+            lax.all_gather(value_a, "sp", axis=0, tiled=True),
+            lax.all_gather(key_b, "sp", axis=0, tiled=True),
+            lax.all_gather(value_b, "sp", axis=0, tiled=True),
+        ),
+    )
+    finished = [
+        (finish_group(states[0], mix_a, head_gain_a), finish_group(states[1], mix_b, head_gain_b))
+        for states in results
+    ]
+    returned = jnp.concatenate([finished[1][0], finished[1][1]], axis=1)
+    for bit in range(levels):
+        returned = partner(returned, "sp", bit)
+    width_a = finished[0][0].shape[1]
+    heads_out_a = jnp.concatenate([finished[0][0], returned[:, :width_a]], axis=0)
+    heads_out_b = jnp.concatenate([finished[0][1], returned[:, width_a:]], axis=0)
+    return heads_out_a, heads_out_b
 
 
 def per_device(
@@ -130,53 +357,22 @@
     expert_up,
     expert_down,
 ):
-    seq_rows = query_a.shape[0]
     sp_ways = lax.axis_size("sp")
-    place = lax.axis_index("sp")
-    positions = place * seq_rows + jnp.arange(seq_rows, dtype=jnp.int32)
-    levels = sp_ways.bit_length() - 1
-    half = seq_rows // 2
-    moved = jnp.concatenate(
-        [query_a[half:].reshape(half, -1), query_b[half:].reshape(half, -1)], axis=1
-    )
-    for bit in range(levels):
-        moved = partner(moved, "sp", bit)
-    split_at = query_a.shape[1] * query_a.shape[2]
-    far_a = moved[:, :split_at].reshape(half, query_a.shape[1], query_a.shape[2])
-    far_b = moved[:, split_at:].reshape(half, query_b.shape[1], query_b.shape[2])
-    far_pos = (sp_ways - 1 - place) * seq_rows + half + jnp.arange(half, dtype=jnp.int32)
-    query_sets = ((query_a[:half], query_b[:half], positions[:half]), (far_a, far_b, far_pos))
-
-    def fold_keys(carry, pieces):
-        return tuple(
-            (set_update(states, queries, pieces) for states, queries in zip(carry, query_sets))
-        )
-
-    initial = tuple(
-        (
-            (empty_group(queries[0], value_a), empty_group(queries[1], value_b))
-            for queries in query_sets
-        )
-    )
-    results = fold_keys(
-        initial,
-        (
-            lax.all_gather(key_a, "sp", axis=0, tiled=True),
-            lax.all_gather(value_a, "sp", axis=0, tiled=True),
-            lax.all_gather(key_b, "sp", axis=0, tiled=True),
-            lax.all_gather(value_b, "sp", axis=0, tiled=True),
-        ),
-    )
-    finished = [
-        (finish_group(states[0], mix_a, head_gain_a), finish_group(states[1], mix_b, head_gain_b))
-        for states in results
-    ]
-    returned = jnp.concatenate([finished[1][0], finished[1][1]], axis=1)
-    for bit in range(levels):
-        returned = partner(returned, "sp", bit)
-    width_a = finished[0][0].shape[1]
-    heads_out_a = jnp.concatenate([finished[0][0], returned[:, :width_a]], axis=0)
-    heads_out_b = jnp.concatenate([finished[0][1], returned[:, width_a:]], axis=0)
+    fits = query_a.shape[1] + query_b.shape[1] == sp_ways
+    fits = fits and query_a.shape[2] == value_a.shape[2] and value_b.shape[2] <= value_a.shape[2]
+    attend = whole_heads if fits else zigzag_heads
+    heads_out_a, heads_out_b = attend(
+        query_a,
+        key_a,
+        value_a,
+        query_b,
+        key_b,
+        value_b,
+        mix_a,
+        mix_b,
+        head_gain_a,
+        head_gain_b,
+    )
     width = resid.shape[1]
     tok_rows = resid.shape[0]
     top_count = route_ids.shape[1]

time: 425 us -> 332 us (0.78)
  matrix products: 78.7 us -> 25.1 us
  Pallas kernels: 0 us -> 47.7 us
  waiting for transfers between devices: 208 us -> 176 us
  other arithmetic: 36.5 us -> 8.33 us
  blocking collectives: 39.1 us -> 12.1 us
  local copies, waits for them, and re-layouts: 27.2 us -> 44.2 us
  starting transfers between devices: 14.5 us -> 4.46 us
  loops' own time: 5.82 us -> 0 us
    dot_general x40 -> x0, matrix products: 53.6 us -> none  [the longest x20 30.7 us: map_update(): jnp.einsum('qhd,khd->hqk', query, keys, preferred_element_type=jnp.float32)]
    pallas_call x0 -> x1, Pallas kernels: none -> 47.7 us  [whole_heads(): pl.pallas_call(functools.partial(heads_kernel, ways, chunk), out_shape=ja...]
    all_gather x2 -> x0, blocking collectives: 26.8 us -> none  [the longest x1 16.1 us: per_device(): lax.all_gather(key_b, 'sp', axis=0, tiled=True)]
    all_gather x2 -> x0, waiting for transfers between devices: 17.1 us -> none  [the longest x1 17.1 us: per_device(): lax.all_gather(value_a, 'sp', axis=0, tiled=True)]
    ppermute x4 -> x0, waiting for transfers between devices: 13.2 us -> none  [partner(): lax.ppermute(value, axis, [(i, i ^ 1 << apart) for i in range(lax.axis_si...]
    add x21 -> x0, other arithmetic: 12.9 us -> none  [the longest x10 12.9 us: map_update(): sums = sums * factor + jnp.sum(weights, axis=2)]
    ppermute x4 -> x0, starting transfers between devices: 9.94 us -> none  [partner(): lax.ppermute(value, axis, [(i, i ^ 1 << apart) for i in range(lax.axis_si...]
    reshape x1 -> x6, local copies, waits for them, and re-layouts: 0.11 us -> 8.12 us  [maps(): jnp.pad(halves, ((0, 0), (0, 0), (0, wide - narrow)))]
  transfers between devices with their start and end apart: 10 -> 4, of which waited for: 8 -> 4; matrix products, arithmetic and copies ran while one was open for 2% -> 0% of each run, Pallas kernels for 0% -> 0%
where the time goes in v1:
time: 332 us; the launch traced here: 331 us
  waiting for transfers between devices  176 us (53%)
  Pallas kernels  47.7 us (14%)
  local copies, waits for them, and re-layouts  44.2 us (13%)
  matrix products  25.1 us (8%)
  between operations  13.5 us (4%)
  blocking collectives  12.1 us (4%)
  other arithmetic  8.33 us (3%)
  starting transfers between devices  4.46 us (1%)
    reduce_scatter x2, waiting for transfers between devices, per_device(): lax.psum_scatter(lax.optimization_barrier(term.astype(jnp.bfloat16)).asty...  103 us
    all_gather x1, waiting for transfers between devices, per_device(): lax.all_gather(arrived.reshape(sp_ways * capacity, width), 'tp', axis=0,...  63.9 us
    pallas_call x1, Pallas kernels, whole_heads(): pl.pallas_call(functools.partial(heads_kernel, ways, chunk), out_shape=ja...  47.7 us
    all_to_all x1, blocking collectives, per_device(): lax.all_to_all(outgoing.reshape(sp_ways, capacity, width), 'sp', split_ax...  12.1 us
    all_to_all x1, waiting for transfers between devices, per_device(): lax.all_to_all(finished_rows, 'sp', split_axis=0, concat_axis=0, tiled=True)  8.81 us
    dot_general x1, matrix products, per_device(): gate = jnp.dot(piece, expert_gate[0], preferred_element_type=jnp.float32)  8.21 us
    reshape x6, local copies, waits for them, and re-layouts, maps(): jnp.pad(halves, ((0, 0), (0, 0), (0, wide - narrow)))  8.12 us
    another operation x9, local copies, waits for them, and re-layouts, whole_heads(): jnp.stack([jnp.pad(gain, (0, wide - value_wide)), jnp.full((wide,), mix[h...  7.26 us
  transfers between devices with their start and end apart: 4, of which 4 were waited for; matrix products, arithmetic and copies ran while one was open for 0% of the time, Pallas kernels for 0%

profile of v1, /device:TPU:0, one launch (start us, length us, event | category | flops | bytes accessed | tf_op | source)
XLA Modules:
  0.0 331.1 jit_solution(275653293570224854)
XLA Ops:
  6.6 1.5 fusion.49
  8.0 1.3 fusion.50
  11.6 1.2 pad.58.clone
  15.4 1.2 pad_bitcast_fusion
  16.6 2.3 fusion.44
  18.9 2.3 fusion.43
  21.2 2.2 fusion.45
  25.7 1.5 fusion.47
  27.9 1.6 copy.55
  29.6 1.5 pad.32
  31.1 1.7 copy.57
  32.7 1.5 pad.33
  34.2 1.7 copy.58
  35.9 1.5 fusion.48
  37.4 1.6 copy.71
  39.0 1.6 copy.70
  45.2 47.7 %shard_map.181 = bf16[4,512,128]{2,1,0:T(8,128)(2,1)S(1)} custom-call(bf16[4,512,384]{2,1,0:T(8,128)(2,1)S(1)} %pad_maximum_fusion.x_ref, f32[8,128]{1,0:T(8,128)S(1)} %pad.36.par_ref), custom_call_target="tpu_custom_call" | custom-call | tf_op jit(solution)/shard_map/pallas_call | solution.py:265
  94.0 2.1 add_convert_fusion
  97.1 34.6 %reduce-scatter.3.cloned.1.call-done = bf16[64,2048]{1,0:T(8,128)(2,1)} async-done(((bf16[512,2048]{1,0:T(8,128)(2,1)}), bf16[64,2048]{1,0:T(8,128)(2,1)}) %reduce-scatter.3.cloned.1.call-update) | async-done | bytes 262160 | tf_op jit(solution)/shard_map/reduce_scatter | solution.py:383
  132.9 1.4 convolution_convert_fusion.1
  134.3 12.1 %all_to_all.10 = bf16[4,48,2048]{2,1,0:T(8,128)(2,1)} all-to-all(bf16[4,48,2048]{2,1,0:T(8,128)(2,1)S(1)} %bitcast.88), channel_id=1, replica_groups=mesh['sp'=4,'tp'=8] {'sp'}, dimensions={0} | all-to-all | bytes 1572864 | tf_op jit(solution)/shard_map/all_to_all | solution.py:399
  146.6 63.9 %all-gather.2.cloned.1.call-done = bf16[1536,2048]{1,0:T(8,128)(2,1)} async-done(((bf16[192,2048]{1,0:T(8,128)(2,1)}), bf16[1536,2048]{1,0:T(8,128)(2,1)}) %all-gather.2.cloned.1.call-update) | async-done | bytes 6291472 | tf_op jit(solution)/shard_map/all_gather | solution.py:402
  210.4 8.2 %fusion.2 = f32[1536,768]{1,0:T(8,128)S(1)} fusion(bf16[1536,2048]{1,0:T(8,128)(2,1)} %all-gather.2.cloned.1.call-done, bf16[1,2048,768]{2,1,0:T(8,128)(2,1)} %param.35), kind=kOutput, calls=%fused_computation.6 | convolution fusion | flops 4831838208 | bytes 14155776 | tf_op jit(solution)/shard_map/dot_general | solution.py:403
  218.7 5.6 %multiply_convert_fusion = bf16[1536,768]{1,0:T(8,128)(2,1)S(1)} fusion(f32[1536,768]{1,0:T(8,128)S(1)} %fusion.2, bf16[1536,2048]{1,0:T(8,128)(2,1)S(1)} %copy-done.14, bf16[1,2048,768]{2,1,0:T(8,128)(2,1)S(1)} %copy-done.15), kind=kOutput, calls=%fused_computation.2 | convolution fusion | flops 4838916096 | bytes 16515072 | tf_op jit(solution)/shard_map/dot_general | solution.py:404
  224.3 7.1 %convolution_convert_fusion = bf16[1536,2048]{1,0:T(8,128)(2,1)} fusion(bf16[1536,768]{1,0:T(8,128)(2,1)S(1)} %multiply_convert_fusion, bf16[1,768,2048]{2,1,0:T(8,128)(2,1)S(1)} %copy-done), kind=kOutput, calls=%fused_computation.1 | convolution fusion | flops 4834983936 | bytes 11796480 | tf_op jit(solution)/shard_map/dot_general | solution.py:406
  231.4 68.5 %reduce-scatter.5.cloned.1.call-done = bf16[192,2048]{1,0:T(8,128)(2,1)} async-done(((bf16[1536,2048]{1,0:T(8,128)(2,1)}), bf16[192,2048]{1,0:T(8,128)(2,1)}) %reduce-scatter.5.cloned.1.call-update) | async-done | bytes 786448 | tf_op jit(solution)/shard_map/reduce_scatter | solution.py:407
  299.9 4.2 %all-to-all-start.1 = ((bf16[4,48,2048]{2,1,0:T(8,128)(2,1)}), bf16[4,48,2048]{2,1,0:T(8,128)(2,1)}, u32[]{:S(2)}, u32[]{:S(2)}) async-start(bf16[4,48,2048]{2,1,0:T(8,128)(2,1)} %bitcast.89), calls=%async_computation.3 | async-start | bytes 1572864 | tf_op jit(solution)/shard_map/all_to_all | solution.py:416
  304.6 8.8 %all-to-all-done.1 = bf16[4,48,2048]{2,1,0:T(8,128)(2,1)} async-done(((bf16[4,48,2048]{2,1,0:T(8,128)(2,1)}), bf16[4,48,2048]{2,1,0:T(8,128)(2,1)}, u32[]{:S(2)}, u32[]{:S(2)}) %all-to-all-start.1) | async-done | bytes 786464 | tf_op jit(solution)/shard_map/all_to_all | solution.py:416
  313.4 3.5 %gather_fusion = bf16[128,2048]{1,0:T(8,128)(2,1)} fusion(bf16[192,2048]{1,0:T(8,128)(2,1)} %bitcast.43, s32[1024]{0:T(1024)S(1)} %pad_clamp_fusion), kind=kCustom, calls=%fused_computation | custom fusion | bytes 1049088 | tf_op jit(solution)/shard_map/jit(_take)/gather | solution.py:417
  316.9 2.2 gather.7
  319.1 3.7 %multiply_reduce_fusion = f32[64,2048]{1,0:T(8,128)S(1)} fusion(bf16[64,2,2048]{2,1,0:T(2,128)(2,1)} %gather.7, pred[64,2]{1,0:T(8,128)(4,1)S(1)} %copy.65, f32[64,2]{1,0:T(8,128)S(1)} %copy.62), kind=kLoop, calls=%fused_computation.10 | loop fusion | flops 917504 | bytes 1049216 | tf_op jit(solution)/shard_map/reduce_sum | solution.py:419
  322.8 1.8 add_convert_fusion.1
  (80 shorter events, 16.1 us)
Async XLA Ops:
  6.5 217.8 %copy-start = (bf16[1,768,2048]{2,1,0:T(8,128)(2,1)S(1)}, bf16[1,768,2048]{2,1,0:T(8,128)(2,1)}, u32[]{:S(2)}) copy-start(bf16[1,768,2048]{2,1,0:T(8,128)(2,1)} %param.37) | copy-start | bytes 9437188
  6.5 16.9 %copy-start.9 = (bf16[512,2,64]{0,2,1:T(8,128)(2,1)S(1)}, bf16[512,2,64]{0,2,1:T(8,128)(2,1)}, u32[]{:S(2)}) copy-start(bf16[512,2,64]{0,2,1:T(8,128)(2,1)} %param.23) | copy-start | bytes 393220
  6.5 34.1 %copy-start.13 = (f32[128]{0:T(128)S(1)}, f32[128]{0:T(128)}, u32[]{:S(2)}) copy-start(f32[128]{0:T(128)} %param.28) | copy-start | bytes 1540
  6.5 125.2 %reduce-scatter.3.cloned.1.call-start = ((), (), s32[]{:S(2)}) async-start(), calls=%async_computation.4 | async-start | bytes 2359296 | tf_op jit(solution)/shard_map/reduce_scatter | solution.py:383
  40.6 4.1 %copy-start.4 = (bf16[512,128]{1,0:T(8,128)(2,1)S(1)}, bf16[512,128]{1,0:T(8,128)(2,1)}, u32[]{:S(2)}) copy-start(bf16[512,128]{1,0:T(8,128)(2,1)} %copy.55) | copy-start | bytes 393220
  40.6 4.2 %copy-start.5 = (bf16[512,128]{1,0:T(8,128)(2,1)S(1)}, bf16[512,128]{1,0:T(8,128)(2,1)}, u32[]{:S(2)}) copy-start(bf16[512,128]{1,0:T(8,128)(2,1)} %copy.57) | copy-start | bytes 393220
  40.6 4.2 %copy-start.6 = (bf16[512,128]{1,0:T(8,128)(2,1)S(1)}, bf16[512,128]{1,0:T(8,128)(2,1)}, u32[]{:S(2)}) copy-start(bf16[512,128]{1,0:T(8,128)(2,1)} %copy.58) | copy-start | bytes 393220
  40.6 4.2 %copy-start.7 = (bf16[512,1,64]{2,0,1:T(8,128)(2,1)S(1)}, bf16[512,1,64]{2,0,1:T(8,128)(2,1)}, u32[]{:S(2)}) copy-start(bf16[512,1,64]{2,0,1:T(8,128)(2,1)} %copy.71) | copy-start | bytes 196612
  40.6 4.2 %copy-start.8 = (bf16[512,1,64]{2,0,1:T(8,128)(2,1)S(1)}, bf16[512,1,64]{2,0,1:T(8,128)(2,1)}, u32[]{:S(2)}) copy-start(bf16[512,1,64]{2,0,1:T(8,128)(2,1)} %copy.70) | copy-start | bytes 196612
  44.9 48.0 %copy-start.2 = (bf16[256,2048]{1,0:T(8,128)(2,1)S(1)}, bf16[256,2048]{1,0:T(8,128)(2,1)}, u32[]{:S(2)}) copy-start(bf16[256,2048]{1,0:T(8,128)(2,1)} %param.30) | copy-start | bytes 3145732
  93.0 1.0 copy-start.3
  94.0 2.2 copy-start.10
  94.0 37.7 %copy-start.1 = (bf16[64,2048]{1,0:T(8,128)(2,1)S(1)}, bf16[64,2048]{1,0:T(8,128)(2,1)}, u32[]{:S(2)}) copy-start(bf16[64,2048]{1,0:T(8,128)(2,1)} %param.19) | copy-start | bytes 786436
  94.0 38.9 %copy-start.11 = (f32[2048]{0:T(1024)S(1)}, f32[2048]{0:T(1024)}, u32[]{:S(2)}) copy-start(f32[2048]{0:T(1024)} %param.32) | copy-start | bytes 24580
  96.1 114.3 %all-gather.2.cloned.1.call-start = ((), (), s32[]{:S(2)}) async-start(), calls=%async_computation.5 | async-start | bytes 7077888 | tf_op jit(solution)/shard_map/all_gather | solution.py:402
  146.3 153.6 %reduce-scatter.5.cloned.1.call-start = ((), (), s32[]{:S(2)}) async-start(), calls=%async_computation.6 | async-start | bytes 7077888 | tf_op jit(solution)/shard_map/reduce_scatter | solution.py:407
  210.4 8.2 %copy-start.14 = (bf16[1536,2048]{1,0:T(8,128)(2,1)S(1)}, bf16[1536,2048]{1,0:T(8,128)(2,1)}, u32[]{:S(2)}) copy-start(bf16[1536,2048]{1,0:T(8,128)(2,1)} %all-gather.2.cloned.1.call-done) | copy-start | bytes 18874372
  210.4 8.2 %copy-start.15 = (bf16[1,2048,768]{2,1,0:T(8,128)(2,1)S(1)}, bf16[1,2048,768]{2,1,0:T(8,128)(2,1)}, u32[]{:S(2)}) copy-start(bf16[1,2048,768]{2,1,0:T(8,128)(2,1)} %param.36) | copy-start | bytes 9437188
  231.4 73.1 %copy-start.12 = (f32[64,2]{0,1:T(2,128)S(1)}, f32[64,2]{0,1:T(2,128)}, u32[]{:S(2)}) copy-start(f32[64,2]{0,1:T(2,128)} %param.34) | copy-start | bytes 1540
  299.9 13.5 %all-to-all-start.1 = ((bf16[4,48,2048]{2,1,0:T(8,128)(2,1)}), bf16[4,48,2048]{2,1,0:T(8,128)(2,1)}, u32[]{:S(2)}, u32[]{:S(2)}) async-start(bf16[4,48,2048]{2,1,0:T(8,128)(2,1)} %bitcast.89), calls=%async_computation.3 | async-start | bytes 1572864 | tf_op jit(solution)/shard_map/all_to_all | solution.py:416
Sparse Core Ops, SparseCore 0:
  96.2 35.4 reduce-scatter.2
  146.5 63.9 all-gather.1
  231.5 68.3 reduce-scatter.4

commit v2 on v1

--- a/solution.py
+++ b/solution.py
@@ -334,6 +334,252 @@
     heads_out_a = jnp.concatenate([finished[0][0], returned[:, :width_a]], axis=0)
     heads_out_b = jnp.concatenate([finished[0][1], returned[:, width_a:]], axis=0)
     return heads_out_a, heads_out_b
+
+
+def remote(src, dst, send_sem, recv_sem, **where):
+    return pltpu.make_async_remote_copy(
+        src_ref=src,
+        dst_ref=dst,
+        send_sem=send_sem,
+        recv_sem=recv_sem,
+        device_id=where,
+        device_id_type=pl.DeviceIdType.MESH,
+    )
+
+
+def greet_routes(places, chips):
+    place, turn = lax.axis_index("sp"), lax.axis_index("tp")
+    chip, core = lax.div(turn, 2), lax.rem(turn, 2)
+    barrier = pltpu.get_barrier_semaphore()
+    peers = [{"tp": 2 * chip + 1 - core}]
+    peers += [{"tp": 2 * lax.rem(chip + apart, chips) + core} for apart in range(1, chips)]
+    peers += [{"sp": lax.rem(place + apart, places)} for apart in range(1, places)]
+    for peer in peers:
+        pl.semaphore_signal(
+            barrier, inc=1, device_id=peer, device_id_type=pl.DeviceIdType.MESH
+        )
+    pl.semaphore_wait(barrier, len(peers))
+
+
+def dispatch_kernel(
+    places, chips, cap, normed_ref, meta_ref, out_ref, near, stage, zs, zr, xs, xr, ps, pr
+):
+    place, turn = lax.axis_index("sp"), lax.axis_index("tp")
+    chip, core = lax.div(turn, 2), lax.rem(turn, 2)
+    other = 2 * chip + 1 - core
+    rows = normed_ref.shape[0]
+    greet_routes(places, chips)
+
+    def near_copy(apart):
+        peer = 2 * lax.rem(chip + apart, chips) + core
+        return remote(normed_ref, near.at[apart], zs.at[apart], zr.at[apart], tp=peer)
+
+    for apart in range(1, chips):
+        near_copy(apart).start()
+
+    def source(apart):
+        return lax.rem(chip + chips - apart, chips)
+
+    def route_copy(apart, away):
+        expert = lax.rem(place + away, places)
+        return remote(
+            stage.at[apart, expert],
+            out_ref.at[core, source(apart), place],
+            xs.at[apart, away],
+            xr.at[apart, away],
+            sp=expert,
+        )
+
+    def pair_copy(apart, away):
+        spot = out_ref.at[core, source(apart), lax.rem(place + places - away, places)]
+        return remote(spot, spot, ps.at[apart, away], pr.at[apart, away], tp=other)
+
+    slot = lax.broadcasted_iota(jnp.int32, (places * cap, rows), 0).astype(jnp.float32)
+    for apart in range(chips):
+        owner = 2 * source(apart) + core
+        spread = jnp.zeros((places * cap, rows), jnp.float32)
+        for which in range(2):
+            own = meta_ref[owner, which : which + 1, 0:rows]
+            spread = spread + jnp.where(slot == own, 1.0, 0.0)
+        if apart:
+            near_copy(apart).wait_recv()
+            piece = near[apart]
+        else:
+            piece = normed_ref[...]
+        sent = jnp.dot(spread.astype(jnp.bfloat16), piece, preferred_element_type=jnp.float32)
+        stage[apart] = sent.astype(jnp.bfloat16).reshape(places, cap, sent.shape[1])
+        for away in range(1, places):
+            route_copy(apart, away).start()
+        out_ref[core, source(apart), place] = stage[apart, place]
+        pair_copy(apart, 0).start()
+    for apart in range(chips):
+        for away in range(1, places):
+            route_copy(apart, away).wait_recv()
+            pair_copy(apart, away).start()
+    for apart in range(chips):
+        if apart:
+            near_copy(apart).wait_send()
+        for away in range(places):
+            if away:
+                route_copy(apart, away).wait_send()
+            pair_copy(apart, away).wait()
+
+
+def combine_kernel(
+    places,
+    chips,
+    cap,
+    term_ref,
+    meta_ref,
+    mixed_ref,
+    out_ref,
+    pair,
+    stage,
+    back,
+    leave,
+    near,
+    ps,
+    pr,
+    xs,
+    xr,
+    zs,
+    zr,
+):
+    place, turn = lax.axis_index("sp"), lax.axis_index("tp")
+    chip, core = lax.div(turn, 2), lax.rem(turn, 2)
+    other = 2 * chip + 1 - core
+    rows = mixed_ref.shape[0]
+    greet_routes(places, chips)
+    order = list(range(1, chips)) + [0]
+
+    def source(apart):
+        return lax.rem(chip + chips - apart, chips)
+
+    def pair_copy(apart):
+        return remote(
+            term_ref.at[1 - core, source(apart)],
+            pair.at[apart],
+            ps.at[apart],
+            pr.at[apart],
+            tp=other,
+        )
+
+    def back_copy(apart, away):
+        peer = lax.rem(place + away, places)
+        return remote(
+            stage.at[apart, peer],
+            back.at[apart, place],
+            xs.at[apart, away],
+            xr.at[apart, away],
+            sp=peer,
+        )
+
+    def near_copy(apart):
+        peer = 2 * source(apart) + core
+        return remote(leave.at[apart], near.at[apart], zs.at[apart], zr.at[apart], tp=peer)
+
+    for apart in order:
+        pair_copy(apart).start()
+    for apart in order:
+        pair_copy(apart).wait_recv()
+        for expert in range(places):
+            stage[apart, expert] = (
+                term_ref[core, source(apart), expert].astype(jnp.float32)
+                + pair[apart, expert].astype(jnp.float32)
+            ).astype(jnp.bfloat16)
+        for away in range(1, places):
+            back_copy(apart, away).start()
+        back[apart, place] = stage[apart, place]
+    slot = lax.broadcasted_iota(jnp.int32, (places * cap, rows), 0).astype(jnp.float32)
+    total = mixed_ref[...]
+    for apart in order:
+        owner = 2 * source(apart) + core
+        gather = jnp.zeros((places * cap, rows), jnp.float32)
+        for which in range(2):
+            own = meta_ref[owner, which : which + 1, 0:rows]
+            weight = meta_ref[owner, which + 2 : which + 3, 0:rows]
+            gather = gather + jnp.where(slot == own, weight, 0.0)
+        high = gather.astype(jnp.bfloat16)
+        low = (gather - high.astype(jnp.float32)).astype(jnp.bfloat16)
+        for away in range(1, places):
+            back_copy(apart, away).wait_recv()
+        held = back[apart].reshape(places * cap, back.shape[3])
+        dims = (((0,), (0,)), ((), ()))
+        part = lax.dot_general(high, held, dims, preferred_element_type=jnp.float32)
+        part = part + lax.dot_general(low, held, dims, preferred_element_type=jnp.float32)
+        if apart:
+            leave[apart] = part.astype(jnp.bfloat16)
+            near_copy(apart).start()
+        else:
+            total = total + part
+    for apart in range(1, chips):
+        near_copy(apart).wait_recv()
+        total = total + near[apart].astype(jnp.float32)
+    out_ref[...] = total.astype(jnp.bfloat16)
+    for apart in range(chips):
+        if apart:
+            near_copy(apart).wait_send()
+        pair_copy(apart).wait_send()
+        for away in range(1, places):
+            back_copy(apart, away).wait_send()
+
+
+def vmem(count):
+    return [pl.BlockSpec(memory_space=pltpu.VMEM)] * count
+
+
+def routed_experts(mixed, normed, meta, capacity, expert_gate, expert_up, expert_down):
+    places, chips = lax.axis_size("sp"), lax.axis_size("tp") // 2
+    rows, width = normed.shape
+    shape = (2, chips, places, capacity, width)
+    sems = pltpu.SemaphoreType.DMA
+    half = pltpu.VMEM((chips, places, capacity, width), jnp.bfloat16)
+    piece_rows = pltpu.VMEM((chips, rows, width), jnp.bfloat16)
+    piece = pl.pallas_call(
+        functools.partial(dispatch_kernel, places, chips, capacity),
+        out_shape=jax.ShapeDtypeStruct(shape, jnp.bfloat16),
+        in_specs=vmem(2),
+        out_specs=vmem(1)[0],
+        scratch_shapes=[
+            piece_rows,
+            half,
+            sems((chips,)),
+            sems((chips,)),
+            sems((chips, places)),
+            sems((chips, places)),
+            sems((chips, places)),
+            sems((chips, places)),
+        ],
+        compiler_params=pltpu.CompilerParams(
+            collective_id=2, has_side_effects=True, vmem_limit_bytes=48 << 20
+        ),
+    )(normed, meta).reshape(-1, width)
+    gate = jnp.dot(piece, expert_gate[0], preferred_element_type=jnp.float32)
+    upward = jnp.dot(piece, expert_up[0], preferred_element_type=jnp.float32)
+    hidden = (jax.nn.silu(gate) * upward).astype(jnp.bfloat16)
+    term = jnp.dot(hidden, expert_down[0], preferred_element_type=jnp.float32)
+    return pl.pallas_call(
+        functools.partial(combine_kernel, places, chips, capacity),
+        out_shape=jax.ShapeDtypeStruct((rows, width), jnp.bfloat16),
+        in_specs=vmem(3),
+        out_specs=vmem(1)[0],
+        scratch_shapes=[
+            half,
+            half,
+            half,
+            piece_rows,
+            piece_rows,
+            sems((chips,)),
+            sems((chips,)),
+            sems((chips, places)),
+            sems((chips, places)),
+            sems((chips,)),
+            sems((chips,)),
+        ],
+        compiler_params=pltpu.CompilerParams(
+            collective_id=3, has_side_effects=True, vmem_limit_bytes=56 << 20
+        ),
+    )(term.astype(jnp.bfloat16).reshape(shape), meta, mixed)
 
 
 def per_device(
@@ -389,6 +635,14 @@
         tiled=True,
     ).astype(jnp.float32)
     normed = rms_scaled(mixed, norm_gain).astype(jnp.bfloat16)
+    tp_ways = lax.axis_size("tp")
+    if top_count == 2 and capacity % 16 == 0 and tok_rows <= 128 and tp_ways % 2 == 0:
+        meta = jnp.concatenate([own_slots.astype(jnp.float32).T, route_weights.T], axis=0)
+        meta = jnp.pad(meta, ((0, 4), (0, 128 - tok_rows)))
+        meta = lax.all_gather(meta, "tp", axis=0)
+        return routed_experts(
+            mixed, normed, meta, capacity, expert_gate, expert_up, expert_down
+        )
     lookup = jnp.arange(sp_ways * capacity, dtype=jnp.int32)[:, None]
     spread = jnp.zeros((sp_ways * capacity, tok_rows), jnp.float32)
     for which in range(top_count):

time: 332 us -> 259 us (0.78)
  waiting for transfers between devices: 176 us -> 18.8 us
  Pallas kernels: 47.7 us -> 143 us
  local copies, waits for them, and re-layouts: 44.2 us -> 39.2 us
  starting transfers between devices: 4.46 us -> 0.01 us
    pallas_call x0 -> x2, Pallas kernels: none -> 95.1 us  [the longest x1 52 us: routed_experts(): pl.pallas_call(functools.partial(combine_kernel, places, chips, capacity)...]
    reduce_scatter x2 -> x1, waiting for transfers between devices: 103 us -> 18.8 us  [per_device(): lax.psum_scatter(lax.optimization_barrier(term.astype(jnp.bfloat16)).asty...]
    all_gather x1 -> x0, waiting for transfers between devices: 63.9 us -> none  [per_device(): lax.all_gather(arrived.reshape(sp_ways * capacity, width), 'tp', axis=0,...]
    all_gather x0 -> x1, blocking collectives: none -> 14.5 us  [per_device(): meta = lax.all_gather(meta, 'tp', axis=0)]
    all_to_all x1 -> x0, blocking collectives: 12.1 us -> none  [per_device(): lax.all_to_all(outgoing.reshape(sp_ways, capacity, width), 'sp', split_ax...]
    all_to_all x1 -> x0, waiting for transfers between devices: 8.81 us -> none  [per_device(): lax.all_to_all(finished_rows, 'sp', split_axis=0, concat_axis=0, tiled=True)]
    gather x2 -> x0, local copies, waits for them, and re-layouts: 5.69 us -> none  [per_device(): jnp.take(back.reshape(sp_ways * capacity, width), own_slots.reshape(-1),...]
    reduce_sum x2 -> x0, other arithmetic: 4.81 us -> none  [the longest x1 3.67 us: per_device(): jnp.sum(route_weights[:, :, None] * picked.astype(jnp.float32), axis=1)]
  transfers between devices with their start and end apart: 4 -> 1, of which waited for: 4 -> 1; matrix products, arithmetic and copies ran while one was open for 0% -> 1% of each run, Pallas kernels for 0% -> 0%
where the time goes in v2:
time: 259 us; the launch traced here: 258 us
  Pallas kernels  143 us (55%)
  local copies, waits for them, and re-layouts  39.2 us (15%)
  matrix products  23 us (9%)
  waiting for transfers between devices  18.8 us (7%)
  blocking collectives  14.5 us (6%)
  between operations  13.7 us (5%)
  other arithmetic  6.23 us (2%)
    pallas_call x1, Pallas kernels, routed_experts(): pl.pallas_call(functools.partial(combine_kernel, places, chips, capacity)...  52 us
    pallas_call x1, Pallas kernels, whole_heads(): pl.pallas_call(functools.partial(heads_kernel, ways, chunk), out_shape=ja...  47.7 us
    pallas_call x1, Pallas kernels, routed_experts(): pl.pallas_call(functools.partial(dispatch_kernel, places, chips, capacity...  43.1 us
    reduce_scatter x1, waiting for transfers between devices, per_device(): lax.psum_scatter(lax.optimization_barrier(term.astype(jnp.bfloat16)).asty...  18.8 us
    all_gather x1, blocking collectives, per_device(): meta = lax.all_gather(meta, 'tp', axis=0)  14.5 us
    reshape x6, local copies, waits for them, and re-layouts, maps(): jnp.pad(halves, ((0, 0), (0, 0), (0, wide - narrow)))  8.13 us
    dot_general x1, matrix products, routed_experts(): gate = jnp.dot(piece, expert_gate[0], preferred_element_type=jnp.float32)  7.55 us
    another operation x9, local copies, waits for them, and re-layouts, whole_heads(): jnp.stack([jnp.pad(gain, (0, wide - value_wide)), jnp.full((wide,), mix[h...  7.22 us
  transfers between devices with their start and end apart: 1, of which 1 were waited for; matrix products, arithmetic and copies ran while one was open for 1% of the time, Pallas kernels for 0%

profile of v2, /device:TPU:0, one launch (start us, length us, event | category | flops | bytes accessed | tf_op | source)
XLA Modules:
  0.0 258.3 jit_solution(1354545310174430072)
XLA Ops:
  8.7 1.3 fusion.42
  10.0 1.2 pad.53.clone
  11.2 1.3 pad.65.clone
  12.5 1.3 fusion.43
  13.9 1.2 pad.57.clone
  15.1 1.3 pad.61.clone
  16.4 1.5 fusion.39
  19.6 1.5 pad.33
  21.1 1.7 copy.74
  22.8 1.5 fusion.40
  24.9 1.7 copy.78
  26.6 1.5 pad.34
  28.1 1.7 copy.75
  29.8 1.5 fusion.41
  31.3 1.6 copy.87
  32.9 1.6 copy.88
  34.5 1.2 fusion.36
  35.6 2.3 fusion.37
  37.9 2.2 fusion.38
  41.0 1.1 copy_bitcast_fusion.2
  44.7 47.7 %shard_map.181 = bf16[4,512,128]{2,1,0:T(8,128)(2,1)S(1)} custom-call(bf16[4,512,384]{2,1,0:T(8,128)(2,1)S(1)} %pad_maximum_fusion.x_ref, f32[8,128]{1,0:T(8,128)S(1)} %pad.40.par_ref), custom_call_target="tpu_custom_call" | custom-call | tf_op jit(solution)/shard_map/pallas_call | solution.py:265
  93.5 2.1 add_convert_fusion
  98.1 14.5 %all-gather = f32[64,128]{1,0:T(8,128)S(1)} all-gather(f32[8,128]{1,0:T(8,128)S(1)} %select_maximum_fusion), channel_id=2, replica_groups=mesh['sp'=4,'tp'=8] {'tp'}, dimensions={0}, use_global_device_ids=true | all-gather | bytes 36864 | tf_op jit(solution)/shard_map/all_gather | solution.py:642
  112.6 18.8 %reduce-scatter.2.cloned.1.call-done = bf16[64,2048]{1,0:T(8,128)(2,1)} async-done(((bf16[512,2048]{1,0:T(8,128)(2,1)}), bf16[64,2048]{1,0:T(8,128)(2,1)}) %reduce-scatter.2.cloned.1.call-update) | async-done | bytes 262160 | tf_op jit(solution)/shard_map/reduce_scatter | solution.py:629
  131.3 1.9 convert_add_fusion
  133.3 1.1 multiply_convert_fusion.1.normed_ref
  134.4 43.1 %shard_map.182 = bf16[2,4,4,48,2048]{4,3,2,1,0:T(8,128)(2,1)} custom-call(bf16[64,2048]{1,0:T(8,128)(2,1)S(1)} %multiply_convert_fusion.1.normed_ref, f32[8,8,128]{2,1,0:T(8,128)S(1)} %bitcast.79), custom_call_target="tpu_custom_call" | custom-call | tf_op jit(solution)/shard_map/pallas_call | solution.py:538
  177.5 7.6 %fusion.2 = f32[1536,768]{1,0:T(8,128)S(1)} fusion(bf16[1536,2048]{1,0:T(8,128)(2,1)} %bitcast.82, bf16[1,2048,768]{2,1,0:T(8,128)(2,1)S(1)} %copy-done.16), kind=kOutput, calls=%fused_computation.5 | convolution fusion | flops 4831838208 | bytes 14155776 | tf_op jit(solution)/shard_map/dot_general | solution.py:557
  185.1 5.6 %multiply_convert_fusion = bf16[1536,768]{1,0:T(8,128)(2,1)S(1)} fusion(f32[1536,768]{1,0:T(8,128)S(1)} %fusion.2, bf16[1536,2048]{1,0:T(8,128)(2,1)S(1)} %bitcast.83, bf16[1,2048,768]{2,1,0:T(8,128)(2,1)S(1)} %copy-done.17), kind=kOutput, calls=%fused_computation.1 | convolution fusion | flops 4838916096 | bytes 16515072 | tf_op jit(solution)/shard_map/dot_general | solution.py:558
  190.7 7.1 %convolution_convert_fusion = bf16[1536,2048]{1,0:T(8,128)(2,1)} fusion(bf16[1536,768]{1,0:T(8,128)(2,1)S(1)} %multiply_convert_fusion, bf16[1,768,2048]{2,1,0:T(8,128)(2,1)S(1)} %copy-done), kind=kOutput, calls=%fused_computation | convolution fusion | flops 4834983936 | bytes 11796480 | tf_op jit(solution)/shard_map/dot_general | solution.py:560
  197.8 52.0 %shard_map.183 = bf16[64,2048]{1,0:T(8,128)(2,1)} custom-call(bf16[2,4,4,48,2048]{4,3,2,1,0:T(8,128)(2,1)} %bitcast.81, f32[8,8,128]{2,1,0:T(8,128)} %bitcast.80, f32[64,2048]{1,0:T(8,128)} %get-tuple-element.5.mixed_ref), custom_call_target="tpu_custom_call" | custom-call | tf_op jit(solution)/shard_map/pallas_call | solution.py:561
  249.8 1.7 copy.99
  (68 shorter events, 11.3 us)
Async XLA Ops:
  6.5 184.2 %copy-start = (bf16[1,768,2048]{2,1,0:T(8,128)(2,1)S(1)}, bf16[1,768,2048]{2,1,0:T(8,128)(2,1)}, u32[]{:S(2)}) copy-start(bf16[1,768,2048]{2,1,0:T(8,128)(2,1)} %param.37) | copy-start | bytes 9437188
  6.5 27.9 %copy-start.3 = (bf16[512,2,128]{2,1,0:T(2,128)(2,1)S(1)}, bf16[512,2,128]{2,1,0:T(2,128)(2,1)}, u32[]{:S(2)}) copy-start(bf16[512,2,128]{2,1,0:T(2,128)(2,1)} %param.20) | copy-start | bytes 786436
  6.5 33.6 %copy-start.15 = (f32[128]{0:T(128)S(1)}, f32[128]{0:T(128)}, u32[]{:S(2)}) copy-start(f32[128]{0:T(128)} %param.28) | copy-start | bytes 1540
  6.5 124.8 %reduce-scatter.2.cloned.1.call-start = ((), (), s32[]{:S(2)}) async-start(), calls=%async_computation.1 | async-start | bytes 2359296 | tf_op jit(solution)/shard_map/reduce_scatter | solution.py:629
  40.1 4.1 %copy-start.7 = (bf16[512,128]{1,0:T(8,128)(2,1)S(1)}, bf16[512,128]{1,0:T(8,128)(2,1)}, u32[]{:S(2)}) copy-start(bf16[512,128]{1,0:T(8,128)(2,1)} %copy.74) | copy-start | bytes 393220
  40.1 4.1 %copy-start.8 = (bf16[512,128]{1,0:T(8,128)(2,1)S(1)}, bf16[512,128]{1,0:T(8,128)(2,1)}, u32[]{:S(2)}) copy-start(bf16[512,128]{1,0:T(8,128)(2,1)} %copy.78) | copy-start | bytes 393220
  40.1 4.2 %copy-start.9 = (bf16[512,128]{1,0:T(8,128)(2,1)S(1)}, bf16[512,128]{1,0:T(8,128)(2,1)}, u32[]{:S(2)}) copy-start(bf16[512,128]{1,0:T(8,128)(2,1)} %copy.75) | copy-start | bytes 393220
  40.1 4.2 %copy-start.10 = (bf16[512,1,64]{2,0,1:T(8,128)(2,1)S(1)}, bf16[512,1,64]{2,0,1:T(8,128)(2,1)}, u32[]{:S(2)}) copy-start(bf16[512,1,64]{2,0,1:T(8,128)(2,1)} %copy.87) | copy-start | bytes 196612
  40.1 4.2 %copy-start.11 = (bf16[512,1,64]{2,0,1:T(8,128)(2,1)S(1)}, bf16[512,1,64]{2,0,1:T(8,128)(2,1)}, u32[]{:S(2)}) copy-start(bf16[512,1,64]{2,0,1:T(8,128)(2,1)} %copy.88) | copy-start | bytes 196612
  44.4 48.0 %copy-start.5 = (bf16[256,2048]{1,0:T(8,128)(2,1)S(1)}, bf16[256,2048]{1,0:T(8,128)(2,1)}, u32[]{:S(2)}) copy-start(bf16[256,2048]{1,0:T(8,128)(2,1)} %param.30) | copy-start | bytes 3145732
  92.5 1.0 copy-start.6
  93.5 2.1 copy-start.13
  93.5 4.5 %copy-start.14 = (f32[64,2]{0,1:T(2,128)S(1)}, f32[64,2]{0,1:T(2,128)}, u32[]{:S(2)}) copy-start(f32[64,2]{0,1:T(2,128)} %param.34) | copy-start | bytes 1540
  93.5 37.8 %copy-start.4 = (bf16[64,2048]{1,0:T(8,128)(2,1)S(1)}, bf16[64,2048]{1,0:T(8,128)(2,1)}, u32[]{:S(2)}) copy-start(bf16[64,2048]{1,0:T(8,128)(2,1)} %param.19) | copy-start | bytes 786436
  95.6 37.7 %copy-start.12 = (f32[2048]{0:T(1024)S(1)}, f32[2048]{0:T(1024)}, u32[]{:S(2)}) copy-start(f32[2048]{0:T(1024)} %param.32) | copy-start | bytes 24580
  112.6 64.9 %copy-start.1 = (f32[64,128]{1,0:T(8,128)}, f32[64,128]{1,0:T(8,128)S(1)}, u32[]{:S(2)}) copy-start(f32[64,128]{1,0:T(8,128)S(1)} %all-gather) | copy-start | bytes 98308
  134.4 43.1 %copy-start.16 = (bf16[1,2048,768]{2,1,0:T(8,128)(2,1)S(1)}, bf16[1,2048,768]{2,1,0:T(8,128)(2,1)}, u32[]{:S(2)}) copy-start(bf16[1,2048,768]{2,1,0:T(8,128)(2,1)} %param.35) | copy-start | bytes 9437188
  177.5 7.6 %copy-start.2 = (bf16[2,4,4,48,2048]{4,3,2,1,0:T(8,128)(2,1)S(1)}, bf16[2,4,4,48,2048]{4,3,2,1,0:T(8,128)(2,1)}, u32[]{:S(2)}) copy-start(bf16[2,4,4,48,2048]{4,3,2,1,0:T(8,128)(2,1)} %shard_map.182) | copy-start | bytes 18874372
  177.5 7.6 %copy-start.17 = (bf16[1,2048,768]{2,1,0:T(8,128)(2,1)S(1)}, bf16[1,2048,768]{2,1,0:T(8,128)(2,1)}, u32[]{:S(2)}) copy-start(bf16[1,2048,768]{2,1,0:T(8,128)(2,1)} %param.36) | copy-start | bytes 9437188
Sparse Core Ops, SparseCore 0:
  95.8 35.5 reduce-scatter.1
